TPU v7x, 32 devices: a whole 2x2x4 slice. The times are simulated.
32 devices in a mesh: grp: 2 (over y), sp: 8 (over z, core), tp: 2 (over x).
Axes of the slice: x: 2, y: 2, z: 4, core: 2. Of those that a mesh axis runs over, the one named last changes fastest.
Arguments:
- queries_a: bfloat16 [4096, 2, 512], P(('grp', 'sp'), None, 'tp'), parts along dimension 0, may hold values from -120 to 120
- keys_a: bfloat16 [4096, 2, 512], P(('grp', 'sp'), None, 'tp'), parts along dimension 0, may hold values from -6 to 6
- values_a: bfloat16 [4096, 1024], P(('grp', 'sp'), 'tp'), parts along dimension 0, may hold values from -6 to 6
- queries_b: bfloat16 [4096, 2, 512], P(('grp', 'sp'), None, 'tp'), parts along dimension 0, may hold values from -120 to 120
- keys_b: bfloat16 [4096, 2, 512], P(('grp', 'sp'), None, 'tp'), parts along dimension 0, may hold values from -6 to 6
- values_b: bfloat16 [4096, 1024], P(('grp', 'sp'), 'tp'), parts along dimension 0, may hold values from -6 to 6
- lambdas: float32 [12], replicated, may hold values from 0.3 to 0.8
- head_gain_a: float32 [256], replicated, may hold values from 0.1 to 1.9
- head_gain_b: float32 [128], replicated, may hold values from 0.1 to 1.9
- out_a: bfloat16 [1024, 2048], P('tp'), may hold values from -0.125 to 0.125
- out_b: bfloat16 [1024, 2048], P('tp'), may hold values from -0.125 to 0.125
- residual: bfloat16 [4096, 2048], P(('grp', 'sp', 'tp')), parts along dimension 0, may hold values from -6 to 6
- gain_mix: float32 [2048], replicated, may hold values from 0.1 to 1.9
- gain_pre: float32 [2048], replicated, may hold values from 0.1 to 1.9
- gain_post: float32 [2048], replicated, may hold values from 0.1 to 1.9
- routes: int32 [4096, 4], P(('grp', 'sp', 'tp')), parts along dimension 0, may hold values from 0 to 7, all different within a row; in each aligned block of 128 rows (0 to 127, 128 to 255, ...) at most 80 rows name the same one
- route_weights: float32 [4096, 4], P(('grp', 'sp', 'tp')), parts along dimension 0, may hold values from 0.05 to 1
- expert_gate: bfloat16 [8, 2048, 2048], P('sp', None, 'tp'), may hold values from -1 to 1
- expert_up: bfloat16 [8, 2048, 2048], P('sp', None, 'tp'), may hold values from -1 to 1
- expert_down: bfloat16 [8, 2048, 2048], P('sp', 'tp'), may hold values from -0.125 to 0.125
Outputs:
- layer_out: bfloat16 [4096, 2048], P(('grp', 'sp', 'tp')), parts along dimension 0
There are 2 independent parts, one for each index of `grp`. A program takes and returns all parts, laid end to end along the dimension named above; an argument that names none is the same for every part. Nothing has to cross between parts.
Inputs may be any that keep to these rules, and one draw needn't show every extreme that they name: `routes`: in each aligned block of 128 rows (the rows of one device) no expert is named by more than 80 rows, a bound that some blocks reach.
All inputs are finite; a program needn't handle non-finite values.
Results may differ from a plain program's by a relative error of at most 0.018.
Values may be sent and summed in bfloat16 or wider, within the bound.
A program may use at most 128 MiB of HBM per device.

v0:
```python
import jax
import jax.numpy as jnp
from jax import lax
from jax.sharding import PartitionSpec as P

HA = 4
DA = 128
DB = 64


def rms_norm(values, gain_vec):
    return values * lax.rsqrt(jnp.mean(values * values, -1, keepdims=True) + 1e-06) * gain_vec


def attend(current, query_rows, key_rows, value_rows, first_row, query_pos, head_size):
    run_max, run_sum, run_acc = current
    key_count = key_rows.shape[0]
    heads = query_rows.shape[2]
    key_view = key_rows.reshape(key_count, 2, heads, head_size)
    value_view = value_rows.reshape(key_count, heads, 2 * head_size)
    key_pos = first_row + jnp.arange(key_count, dtype=jnp.int32)
    visible = (key_pos[None, :] <= query_pos[:, None])[None, :, None, :]
    scores = jnp.einsum(
        "qmhd,kmhd->mqhk", query_rows, key_view, preferred_element_type=jnp.float32
    ) * head_size ** (-0.5)
    scores = jnp.where(visible, scores, -1e30)
    new_max = jnp.maximum(run_max, jnp.max(scores, -1))
    exp_terms = jnp.where(visible, jnp.exp(scores - new_max[..., None]), 0.0)
    rescale = jnp.exp(run_max - new_max)
    run_sum = run_sum * rescale + jnp.sum(exp_terms, -1)
    run_acc = run_acc * rescale[..., None] + jnp.einsum(
        "mqhk,khe->mqhe",
        exp_terms.astype(jnp.bfloat16),
        value_view,
        preferred_element_type=jnp.float32,
    )
    return (new_max, run_sum, run_acc)


def fresh_state(length, heads, head_size):
    return (
        jnp.full((2, length, heads), -1e30, jnp.float32),
        jnp.zeros((2, length, heads), jnp.float32),
        jnp.zeros((2, length, heads, 2 * head_size), jnp.float32),
    )


def finish(current, weights_two, gain_vec):
    run_max, run_sum, run_acc = current
    mixture = (
        run_acc[0] / run_sum[0][..., None]
        - weights_two[None, :, None] * run_acc[1] / run_sum[1][..., None]
    )
    normed = rms_norm(mixture, gain_vec)
    return normed.reshape(normed.shape[0], -1).astype(jnp.bfloat16)


def slot_numbers(flat_ids, experts):
    onehot = (flat_ids[:, None] == jnp.arange(experts, dtype=jnp.int32)[None, :]).astype(jnp.int32)
    before = jnp.cumsum(onehot, 0) - onehot
    return jnp.sum(before * onehot, 1)


def send_matrix(route_rows, experts, capacity):
    groups, sub_rows, top_count = route_rows.shape
    slot_ids = jax.vmap(lambda flat_ids: slot_numbers(flat_ids, experts))(
        route_rows.reshape(groups, -1)
    )
    group_ids = jnp.arange(groups, dtype=jnp.int32)[:, None]
    row_ids = (
        route_rows.reshape(groups, -1) * (groups * capacity) + group_ids * capacity + slot_ids
    ).reshape(-1)
    col_ids = jnp.broadcast_to(
        group_ids[:, :, None] * sub_rows + jnp.arange(sub_rows, dtype=jnp.int32)[None, :, None],
        route_rows.shape,
    ).reshape(-1)
    row_hot = (
        row_ids[:, None] == jnp.arange(experts * groups * capacity, dtype=jnp.int32)[None, :]
    ).astype(jnp.bfloat16)
    col_hot = (col_ids[:, None] == jnp.arange(groups * sub_rows, dtype=jnp.int32)[None, :]).astype(
        jnp.bfloat16
    )
    return jnp.einsum("ar,ac->rc", row_hot, col_hot, preferred_element_type=jnp.float32).astype(
        jnp.bfloat16
    )


def back_matrix(route_rows, route_weights, experts, capacity):
    sub_rows, top_count = route_rows.shape
    slot_ids = slot_numbers(route_rows.reshape(-1), experts)
    row_ids = route_rows.reshape(-1) * capacity + slot_ids
    col_ids = jnp.repeat(jnp.arange(sub_rows, dtype=jnp.int32), top_count)
    row_hot = (row_ids[:, None] == jnp.arange(experts * capacity, dtype=jnp.int32)[None, :]).astype(
        jnp.float32
    )
    tok_weighted = (col_ids[:, None] == jnp.arange(sub_rows, dtype=jnp.int32)[None, :]).astype(
        jnp.float32
    ) * route_weights.reshape(-1)[:, None]
    return jnp.einsum("at,ar->tr", tok_weighted, row_hot, precision=lax.Precision.HIGHEST)


def per_device(
    queries_a,
    keys_a,
    values_a,
    queries_b,
    keys_b,
    values_b,
    lambdas,
    head_gain_a,
    head_gain_b,
    out_a,
    out_b,
    residual,
    gain_mix,
    gain_pre,
    gain_post,
    routes,
    route_weights,
    expert_gate,
    expert_up,
    expert_down,
):
    length = queries_a.shape[0]
    heads_a = queries_a.shape[2] // DA
    heads_b = queries_b.shape[2] // DB
    head_slot = lax.axis_index("tp")
    seq_slot = lax.axis_index("sp")
    lambda_a = lax.dynamic_slice_in_dim(lambdas, head_slot * heads_a, heads_a)
    lambda_b = lax.dynamic_slice_in_dim(lambdas, HA + head_slot * heads_b, heads_b)
    groups = [
        (
            queries_a.reshape(length, 2, heads_a, DA),
            queries_b.reshape(length, 2, heads_b, DB),
            seq_slot * length + jnp.arange(length, dtype=jnp.int32),
            seq_slot * length + length - 1,
        )
    ]
    initial = tuple(
        (
            (
                fresh_state(group[2].shape[0], heads_a, DA),
                fresh_state(group[2].shape[0], heads_b, DB),
            )
            for group in groups
        )
    )
    pieces = (
        lax.all_gather(keys_a, "sp", axis=0, tiled=True),
        lax.all_gather(values_a, "sp", axis=0, tiled=True),
        lax.all_gather(keys_b, "sp", axis=0, tiled=True),
        lax.all_gather(values_b, "sp", axis=0, tiled=True),
    )
    key_count = pieces[0].shape[0]
    span_rows = 1024

    def one_span(span_index, carried):
        offset = span_index * span_rows
        parts = tuple(
            (lax.dynamic_slice_in_dim(piece_part, offset, span_rows, 0) for piece_part in pieces)
        )
        group_qa, group_qb, group_pos, group_last = groups[0]

        def compute(inner, group_qa=group_qa, group_qb=group_qb, group_pos=group_pos):
            return (
                attend(inner[0], group_qa, parts[0], parts[1], offset, group_pos, DA),
                attend(inner[1], group_qb, parts[2], parts[3], offset, group_pos, DB),
            )

        updated = [lax.cond(offset <= group_last, compute, lambda inner: inner, carried[0])]
        return tuple(updated)

    final_state = lax.fori_loop(0, key_count // span_rows, one_span, initial)
    heads_out_a = finish(final_state[0][0], lambda_a, head_gain_a)
    heads_out_b = finish(final_state[0][1], lambda_b, head_gain_b)
    mixed_rows = lax.psum_scatter(
        (
            jnp.dot(heads_out_a, out_a, preferred_element_type=jnp.float32)
            + jnp.dot(heads_out_b, out_b, preferred_element_type=jnp.float32)
        ).astype(jnp.bfloat16),
        "tp",
        scatter_dimension=0,
        tiled=True,
    ).astype(jnp.float32)
    after_mix = (residual.astype(jnp.float32) + rms_norm(mixed_rows, gain_mix)).astype(jnp.bfloat16)
    normed = rms_norm(after_mix.astype(jnp.float32), gain_pre).astype(jnp.bfloat16)
    experts = lax.axis_size("sp")
    sub_rows = residual.shape[0]
    top_count = routes.shape[1]
    capacity = min(sub_rows, (5 * sub_rows * top_count + 4 * experts - 1) // (4 * experts))
    width = residual.shape[1]
    outgoing = jnp.dot(
        send_matrix(routes[None], experts, capacity), normed, preferred_element_type=jnp.float32
    ).astype(jnp.bfloat16)
    outgoing = outgoing.reshape(experts, capacity, width)
    arrived = lax.all_to_all(outgoing, "sp", split_axis=0, concat_axis=0, tiled=True)
    sources, slot_count, columns = arrived.shape
    piece_rows = lax.all_gather(arrived.reshape(-1, columns), "tp", axis=0, tiled=True)
    gate_pre = jnp.dot(piece_rows, expert_gate[0], preferred_element_type=jnp.float32)
    up_pre = jnp.dot(piece_rows, expert_up[0], preferred_element_type=jnp.float32)
    glu_part = jnp.minimum(gate_pre, 7.0)
    lin_part = jnp.clip(up_pre, -7.0, 7.0)
    hidden = (glu_part * jax.nn.sigmoid(1.702 * glu_part) * (lin_part + 1.0)).astype(jnp.bfloat16)
    partials = jnp.dot(hidden, expert_down[0], preferred_element_type=jnp.float32)
    mine = lax.psum_scatter(partials.astype(jnp.bfloat16), "tp", scatter_dimension=0, tiled=True)
    results = mine.reshape(sources, slot_count, columns)
    returned = lax.all_to_all(results, "sp", split_axis=0, concat_axis=0, tiled=True)
    combine = back_matrix(routes, route_weights, experts, capacity)
    routed = jnp.dot(
        combine,
        returned.reshape(-1, width).astype(jnp.float32),
        precision=lax.Precision.HIGHEST,
        preferred_element_type=jnp.float32,
    )
    return (after_mix.astype(jnp.float32) + rms_norm(routed, gain_post)).astype(jnp.bfloat16)


def solution(mesh):
    in_specs = (
        P(("grp", "sp"), None, "tp"),
        P(("grp", "sp"), None, "tp"),
        P(("grp", "sp"), "tp"),
        P(("grp", "sp"), None, "tp"),
        P(("grp", "sp"), None, "tp"),
        P(("grp", "sp"), "tp"),
        P(),
        P(),
        P(),
        P("tp", None),
        P("tp", None),
        P(("grp", "sp", "tp"), None),
        P(),
        P(),
        P(),
        P(("grp", "sp", "tp"), None),
        P(("grp", "sp", "tp"), None),
        P("sp", None, "tp"),
        P("sp", None, "tp"),
        P("sp", "tp", None),
    )
    out_specs = P(("grp", "sp", "tp"), None)
    return jax.shard_map(
        per_device, mesh=mesh, in_specs=in_specs, out_specs=out_specs, check_vma=False
    )
```

profile of v0, /device:TPU:0, one launch (start us, length us, event | category | flops | bytes accessed | tf_op | source)
XLA Modules:
  0.0 503.5 jit_solution(3561112254705816321)
XLA Ops:
  6.6 2.0 copy.36
  8.6 1.8 copy.38
  10.5 1.8 copy.39
  12.4 1.8 copy.41
  17.5 24.9 %all-gather.6.cloned.1.call-done = bf16[2048,2,256]{0,2,1:T(8,128)(2,1)} async-done(((bf16[256,2,256]{0,2,1:T(8,128)(2,1)}), bf16[2048,2,256]{0,2,1:T(8,128)(2,1)}) %all-gather.6.cloned.1.call-update) | async-done | bytes 2097168 | tf_op jit(solution)/shard_map/all_gather | solution.py:149
  42.4 31.3 %all-gather.8.cloned.1.call-done = bf16[2048,512]{0,1:T(8,128)(2,1)} async-done(((bf16[256,512]{0,1:T(8,128)(2,1)}), bf16[2048,512]{0,1:T(8,128)(2,1)}) %all-gather.8.cloned.1.call-update) | async-done | bytes 2097168 | tf_op jit(solution)/shard_map/all_gather | solution.py:150
  73.7 31.3 %all-gather.10.cloned.1.call-done = bf16[2048,2,256]{0,2,1:T(8,128)(2,1)} async-done(((bf16[256,2,256]{0,2,1:T(8,128)(2,1)}), bf16[2048,2,256]{0,2,1:T(8,128)(2,1)}) %all-gather.10.cloned.1.call-update) | async-done | bytes 2097168 | tf_op jit(solution)/shard_map/all_gather | solution.py:151
  104.9 31.1 %all-gather.12.cloned.1.call-done = bf16[2048,512]{0,1:T(8,128)(2,1)} async-done(((bf16[256,512]{0,1:T(8,128)(2,1)}), bf16[2048,512]{0,1:T(8,128)(2,1)}) %all-gather.12.cloned.1.call-update) | async-done | bytes 2097168 | tf_op jit(solution)/shard_map/all_gather | solution.py:152
  137.3 13.8 %while.24 = (s32[]{:T(128)}, f32[2,256,2]{1,2,0:T(2,128)S(1)}, f32[2,256,2]{1,2,0:T(2,128)S(1)}, f32[2,256,2,256]{3,1,0,2:T(8,128)S(1)}, f32[2,256,4]{1,2,0:T(4,...) while((s32[]{:T(128)}, f32[2,256,2]{1,2,0:T(2,128)S(1)}, ...), condition=%wide.region_7.8_spmd.clone, body=%wide.region_0.7_spmd.clone.sunk | while | flops 1640242432 | bytes 83845752 | solution.py:173
  137.3 13.8 %conditional.3 = ((f32[2,256,2]{1,2,0:T(2,128)S(1)}, f32[2,256,2]{1,2,0:T(2,128)S(1)}, f32[2,256,2,256]{3,1,0,2:T(8,128)S(1)}, f32[2,256,4]{1,2,0:T(4,128)S(1)},...) conditional(s32[]{:T(128)} %convert_element_type.151, (f32[2,256,2]{1,2,0:T(2,128)S(1)}, ...), branch_computations={%region_1.0_spmd, %region_2.6_spmd} | conditional | flops 1640242432 | bytes 83844368 | solution.py:170
  137.5 1.8 constant_dynamic-slice_fusion.1
  142.7 1.3 fusion.15
  144.1 1.5 fusion.2
  145.6 2.3 fusion.3
  148.0 2.0 fusion.21
  152.4 2.3 fusion.84
  154.7 1.4 fusion.65
  156.0 1.6 copy.45
  157.9 1.5 fusion.57
  160.4 1.7 fusion.34
  162.6 1.3 reduce-window.16
  165.9 29.2 %reduce-scatter.3.cloned.1.call-done = bf16[128,2048]{1,0:T(8,128)(2,1)} async-done(((bf16[256,2048]{1,0:T(8,128)(2,1)}), bf16[128,2048]{1,0:T(8,128)(2,1)}) %reduce-scatter.3.cloned.1.call-update) | async-done | bytes 524304 | tf_op jit(solution)/shard_map/reduce_scatter | solution.py:176
  196.4 1.5 fusion.42
  197.8 3.0 convolution_convert_fusion.1
  200.8 65.0 %all_to_all.10 = bf16[8,80,2048]{2,1,0:T(8,128)(2,1)} all-to-all(bf16[8,80,2048]{2,1,0:T(8,128)(2,1)} %bitcast.199), channel_id=1, replica_groups=mesh['grp'=2,'sp'=8,'tp'=2] {'sp'}, dimensions={0} | all-to-all | bytes 5242880 | tf_op jit(solution)/shard_map/all_to_all | solution.py:196
  265.9 66.6 %all-gather.14.cloned.1.call-done = bf16[1280,2048]{1,0:T(8,128)(2,1)} async-done(((bf16[640,2048]{1,0:T(8,128)(2,1)}), bf16[1280,2048]{1,0:T(8,128)(2,1)}) %all-gather.14.cloned.1.call-update) | async-done | bytes 5242896 | tf_op jit(solution)/shard_map/all_gather | solution.py:198
  332.5 10.2 %fusion.26 = f32[1280,1024]{1,0:T(8,128)} fusion(bf16[1280,2048]{1,0:T(8,128)(2,1)} %all-gather.14.cloned.1.call-done, bf16[1,2048,1024]{2,1,0:T(8,128)(2,1)} %param.41), kind=kOutput, calls=%fused_computation.34 | convolution fusion | flops 5368709120 | bytes 14680064 | tf_op jit(solution)/shard_map/dot_general | solution.py:199
  342.7 18.7 %convolution_convert_fusion = bf16[1280,2048]{1,0:T(8,128)(2,1)} fusion(bf16[1,1024,2048]{2,1,0:T(8,128)(2,1)} %param.43, f32[1280,1024]{1,0:T(8,128)} %fusion.26, bf16[1280,2048]{1,0:T(8,128)(2,1)} %all-gather.14.cloned.1.call-done, bf16[1,2048,1024]{2,1,0:T(8,128)(2,1)} %param.42), kind=kOutput, calls=%fused_computation.30 | convolution fusion | flops 10753146880 | bytes 24117248 | tf_op jit(solution)/shard_map/dot_general | solution.py:204
  361.4 65.9 %reduce-scatter.5.cloned.1.call-done = bf16[640,2048]{1,0:T(8,128)(2,1)} async-done(((bf16[1280,2048]{1,0:T(8,128)(2,1)}), bf16[640,2048]{1,0:T(8,128)(2,1)}) %reduce-scatter.5.cloned.1.call-update) | async-done | bytes 2621456 | tf_op jit(solution)/shard_map/reduce_scatter | solution.py:205
  427.3 4.7 all-to-all-start.1
  433.1 59.3 %all-to-all-done.1 = bf16[8,80,2048]{2,1,0:T(8,128)(2,1)} async-done(((bf16[8,80,2048]{2,1,0:T(8,128)(2,1)}), bf16[8,80,2048]{2,1,0:T(8,128)(2,1)}, u32[]{:S(2)}, u32[]{:S(2)}) %all-to-all-start.1) | async-done | bytes 2621472 | tf_op jit(solution)/shard_map/all_to_all | solution.py:207
  492.4 3.2 multiply_reduce_fusion
  (117 shorter events, 17.5 us)
Async XLA Ops:
  6.5 152.9 %copy-start = (bf16[512,2048]{1,0:T(8,128)(2,1)S(1)}, bf16[512,2048]{1,0:T(8,128)(2,1)}, u32[]{:S(2)}) copy-start(bf16[512,2048]{1,0:T(8,128)(2,1)} %param.33) | copy-start | bytes 6291460
  6.5 9.7 %copy-start.9 = (bf16[256,2,256]{2,1,0:T(2,128)(2,1)S(1)}, bf16[256,2,256]{2,1,0:T(2,128)(2,1)}, u32[]{:S(2)}) copy-start(bf16[256,2,256]{2,1,0:T(2,128)(2,1)} %param.27) | copy-start | bytes 786436
  6.5 10.6 %copy-start.15 = (f32[256]{0:T(256)S(1)}, f32[256]{0:T(256)}, u32[]{:S(2)}) copy-start(f32[256]{0:T(256)} %param.31) | copy-start | bytes 3076
  6.5 10.6 %copy-start.17 = (f32[12]{0:T(128)S(1)}, f32[12]{0:T(128)}, u32[]{:S(2)}) copy-start(f32[12]{0:T(128)} %param.30) | copy-start | bytes 148
  6.5 10.8 %copy-start.16 = (f32[128]{0:T(128)S(1)}, f32[128]{0:T(128)}, u32[]{:S(2)}) copy-start(f32[128]{0:T(128)} %param.32) | copy-start | bytes 1540
  6.5 35.8 %all-gather.6.cloned.1.call-start = ((), (), s32[]{:S(2)}) async-start(), calls=%async_computation.4 | async-start | bytes 2359296 | tf_op jit(solution)/shard_map/all_gather | solution.py:149
  8.6 65.1 %all-gather.8.cloned.1.call-start = ((), (), s32[]{:S(2)}) async-start(), calls=%async_computation.5 | async-start | bytes 2359296 | tf_op jit(solution)/shard_map/all_gather | solution.py:150
  10.5 94.5 %all-gather.10.cloned.1.call-start = ((), (), s32[]{:S(2)}) async-start(), calls=%async_computation.6 | async-start | bytes 2359296 | tf_op jit(solution)/shard_map/all_gather | solution.py:151
  12.4 123.7 %all-gather.12.cloned.1.call-start = ((), (), s32[]{:S(2)}) async-start(), calls=%async_computation.7 | async-start | bytes 2359296 | tf_op jit(solution)/shard_map/all_gather | solution.py:152
  14.3 180.8 %reduce-scatter.3.cloned.1.call-start = ((), (), s32[]{:S(2)}) async-start(), calls=%async_computation.8 | async-start | bytes 1572864 | tf_op jit(solution)/shard_map/reduce_scatter | solution.py:176
  137.5 1.8 copy-start.3
  140.3 1.6 copy-start.1
  140.3 2.2 copy-start.2
  142.5 1.6 copy-start.4
  145.6 2.4 copy-start.5
  150.0 1.0 copy-start.6
  157.7 2.7 copy-start.7
  160.2 2.0 copy-start.13
  160.2 36.2 %copy-start.8 = (bf16[128,2048]{1,0:T(8,128)(2,1)S(1)}, bf16[128,2048]{1,0:T(8,128)(2,1)}, u32[]{:S(2)}) copy-start(bf16[128,2048]{1,0:T(8,128)(2,1)} %param.35) | copy-start | bytes 1572868
  160.2 36.2 %copy-start.10 = (f32[2048]{0:T(1024)S(1)}, f32[2048]{0:T(1024)}, u32[]{:S(2)}) copy-start(f32[2048]{0:T(1024)} %param.36) | copy-start | bytes 24580
  160.4 37.4 %copy-start.11 = (f32[2048]{0:T(1024)S(1)}, f32[2048]{0:T(1024)}, u32[]{:S(2)}) copy-start(f32[2048]{0:T(1024)} %param.37) | copy-start | bytes 24580
  162.2 170.3 %all-gather.14.cloned.1.call-start = ((), (), s32[]{:S(2)}) async-start(), calls=%async_computation.9 | async-start | bytes 7864320 | tf_op jit(solution)/shard_map/all_gather | solution.py:198
  265.8 161.5 %reduce-scatter.5.cloned.1.call-start = ((), (), s32[]{:S(2)}) async-start(), calls=%async_computation.10 | async-start | bytes 7864320 | tf_op jit(solution)/shard_map/reduce_scatter | solution.py:205
  361.4 70.7 %copy-start.14 = (f32[128,4]{0,1:T(4,128)S(1)}, f32[128,4]{0,1:T(4,128)}, u32[]{:S(2)}) copy-start(f32[128,4]{0,1:T(4,128)} %param.40) | copy-start | bytes 6148
  427.3 68.3 %copy-start.12 = (f32[2048]{0:T(1024)S(1)}, f32[2048]{0:T(1024)}, u32[]{:S(2)}) copy-start(f32[2048]{0:T(1024)} %param.38) | copy-start | bytes 24580
  427.3 65.1 %all-to-all-start.1 = ((bf16[8,80,2048]{2,1,0:T(8,128)(2,1)}), bf16[8,80,2048]{2,1,0:T(8,128)(2,1)}, u32[]{:S(2)}, u32[]{:S(2)}) async-start(bf16[8,80,2048]{2,1,0:T(8,128)(2,1)} %bitcast.202), calls=%async_computation.3 | async-start | bytes 5242880 | tf_op jit(solution)/shard_map/all_to_all | solution.py:207
Sparse Core Ops, SparseCore 0:
  8.9 33.3 all-gather.5
  44.0 29.6 all-gather.7
  75.3 29.6 all-gather.9
  106.4 29.6 all-gather.11
  162.3 32.7 reduce-scatter.2
  266.0 66.4 all-gather.13
  361.5 65.7 reduce-scatter.4
where the time goes:
time: 504 us
  waiting for transfers between devices  340 us (67%)
  blocking collectives  65 us (13%)
  matrix products  44.2 us (9%)
  local copies, waits for them, and re-layouts  22.1 us (4%)
  between operations  13.8 us (3%)
  other arithmetic  13.5 us (3%)
  starting transfers between devices  5.04 us (1%)
    all_gather x1, waiting for transfers between devices, per_device(): lax.all_gather(arrived.reshape(-1, columns), 'tp', axis=0, tiled=True)  66.6 us
    reduce_scatter x1, waiting for transfers between devices, per_device(): lax.psum_scatter(partials.astype(jnp.bfloat16), 'tp', scatter_dimension=0...  65.9 us
    all_to_all x1, blocking collectives, per_device(): lax.all_to_all(outgoing, 'sp', split_axis=0, concat_axis=0, tiled=True)  65 us
    all_to_all x1, waiting for transfers between devices, per_device(): lax.all_to_all(results, 'sp', split_axis=0, concat_axis=0, tiled=True)  59.3 us
    all_gather x1, waiting for transfers between devices, per_device(): lax.all_gather(values_a, 'sp', axis=0, tiled=True)  31.3 us
    all_gather x1, waiting for transfers between devices, per_device(): lax.all_gather(keys_b, 'sp', axis=0, tiled=True)  31.3 us
    all_gather x1, waiting for transfers between devices, per_device(): lax.all_gather(values_b, 'sp', axis=0, tiled=True)  31.1 us
    reduce_scatter x1, waiting for transfers between devices, per_device(): lax.psum_scatter((jnp.dot(heads_out_a, out_a, preferred_element_type=jnp....  29.2 us
  transfers between devices with their start and end apart: 8, of which 8 were waited for; matrix products, arithmetic and copies ran while one was open for 3% of the time, Pallas kernels for 0%

commit v1 on v0

--- a/solution.py
+++ b/solution.py
@@ -6,6 +6,33 @@
 HA = 4
 DA = 128
 DB = 64
+
+
+def racks_watch(xin, which_axis, array_dim):
+    kept_arr = lax.axis_size(which_axis)
+    d_next = lax.axis_index(which_axis)
+    latest, o_now, local_next = (kept_arr, d_next, xin.shape[array_dim])
+    made = [(hop_no, (hop_no + 1) % latest) for hop_no in range(latest)]
+    tray = [(hop_no, (hop_no - 1) % latest) for hop_no in range(latest)]
+    block_out = jnp.zeros(
+        (*xin.shape[:array_dim], latest * local_next, *xin.shape[array_dim + 1 :]), xin.dtype
+    )
+    block_out = lax.dynamic_update_slice_in_dim(block_out, xin, o_now * local_next, axis=array_dim)
+    s_next = moved = xin
+    odd = latest // 2
+    t = 1
+    while t < odd + 1:
+        s_next = lax.ppermute(s_next, which_axis, made)
+        block_out = lax.dynamic_update_slice_in_dim(
+            block_out, s_next, (o_now - t) % latest * local_next, axis=array_dim
+        )
+        if t < latest - odd:
+            moved = lax.ppermute(moved, which_axis, tray)
+            block_out = lax.dynamic_update_slice_in_dim(
+                block_out, moved, (o_now + t) % latest * local_next, axis=array_dim
+            )
+        t += 1
+    return block_out
 
 
 def rms_norm(values, gain_vec):
@@ -149,7 +176,7 @@
         lax.all_gather(keys_a, "sp", axis=0, tiled=True),
         lax.all_gather(values_a, "sp", axis=0, tiled=True),
         lax.all_gather(keys_b, "sp", axis=0, tiled=True),
-        lax.all_gather(values_b, "sp", axis=0, tiled=True),
+        racks_watch(values_b, "sp", 0),
     )
     key_count = pieces[0].shape[0]
     span_rows = 1024

time: 504 us -> 485 us (0.962)
  waiting for transfers between devices: 340 us -> 291 us
  starting transfers between devices: 5.04 us -> 23.7 us
  local copies, waits for them, and re-layouts: 22.1 us -> 33.2 us
    all_gather x1 -> x0, waiting for transfers between devices: 31.1 us -> none  [per_device(): lax.all_gather(values_b, 'sp', axis=0, tiled=True)]
    all_gather x1, waiting for transfers between devices: 24.9 us -> 0.01 us  [per_device(): lax.all_gather(keys_a, 'sp', axis=0, tiled=True)]
    ppermute x0 -> x7, starting transfers between devices: none -> 18.5 us  [the longest x3 10.9 us: racks_watch(): moved = lax.ppermute(moved, which_axis, tray)]
    ppermute x0 -> x7, waiting for transfers between devices: none -> 11.2 us  [the longest x3 6.5 us: racks_watch(): moved = lax.ppermute(moved, which_axis, tray)]
    dynamic_update_slice x0 -> x8, local copies, waits for them, and re-layouts: none -> 6.02 us  [the longest x4 3.01 us: racks_watch(): lax.dynamic_update_slice_in_dim(block_out, s_next, (o_now - t) % latest *...]
    unnamed x37 -> x29, local copies, waits for them, and re-layouts: 10.6 us -> 11.4 us
  transfers between devices with their start and end apart: 8 -> 14, of which waited for: 8 -> 10; matrix products, arithmetic and copies ran while one was open for 3% -> 5% of each run, Pallas kernels for 0% -> 0%
where the time goes in v1:
time: 485 us
  waiting for transfers between devices  291 us (60%)
  blocking collectives  65 us (13%)
  matrix products  44.2 us (9%)
  local copies, waits for them, and re-layouts  33.2 us (7%)
  starting transfers between devices  23.7 us (5%)
  between operations  13.7 us (3%)
  other arithmetic  13.3 us (3%)
    all_gather x1, waiting for transfers between devices, per_device(): lax.all_gather(arrived.reshape(-1, columns), 'tp', axis=0, tiled=True)  66.6 us
    reduce_scatter x1, waiting for transfers between devices, per_device(): lax.psum_scatter(partials.astype(jnp.bfloat16), 'tp', scatter_dimension=0...  65.9 us
    all_to_all x1, blocking collectives, per_device(): lax.all_to_all(outgoing, 'sp', split_axis=0, concat_axis=0, tiled=True)  65 us
    all_to_all x1, waiting for transfers between devices, per_device(): lax.all_to_all(results, 'sp', split_axis=0, concat_axis=0, tiled=True)  59.3 us
    all_gather x1, waiting for transfers between devices, per_device(): lax.all_gather(keys_b, 'sp', axis=0, tiled=True)  31.3 us
    reduce_scatter x1, waiting for transfers between devices, per_device(): lax.psum_scatter((jnp.dot(heads_out_a, out_a, preferred_element_type=jnp....  29.8 us
    all_gather x1, waiting for transfers between devices, per_device(): lax.all_gather(values_a, 'sp', axis=0, tiled=True)  27.1 us
    dot_general x1, matrix products, per_device(): jnp.dot(hidden, expert_down[0], preferred_element_type=jnp.float32)  18.7 us
  transfers between devices with their start and end apart: 14, of which 10 were waited for; matrix products, arithmetic and copies ran while one was open for 5% of the time, Pallas kernels for 0%

profile of v1, /device:TPU:0, one launch (start us, length us, event | category | flops | bytes accessed | tf_op | source)
XLA Modules:
  0.0 484.5 jit_solution(8779997499716233622)
XLA Ops:
  6.5 2.0 copy.36
  8.6 1.8 copy.38
  10.5 1.8 copy.39
  14.0 4.1 collective-permute-start.1
  22.3 6.5 %collective-permute-done.1 = bf16[256,512]{0,1:T(8,128)(2,1)S(1)} collective-permute-done((bf16[256,512]{0,1:T(8,128)(2,1)S(1)}, bf16[256,512]{0,1:T(8,128)(2,1)S(1)}, u32[]{:S(2)}, u32[]{:S(2)}) %collective-permute-start.1) | collective-permute-done | bytes 262176 | tf_op jit(solution)/shard_map/ppermute | solution.py:30
  28.8 3.7 collective-permute-start.3
  32.6 1.6 broadcast_in_dim.120
  36.9 1.8 copy.40
  38.7 2.6 collective-permute-start.4
  42.8 3.1 collective-permute-start.5
  47.5 4.4 collective-permute-start.6
  54.1 2.5 collective-permute-done.6
  57.4 27.1 %all-gather.7.cloned.1.call-done = bf16[2048,512]{0,1:T(8,128)(2,1)} async-done(((bf16[256,512]{0,1:T(8,128)(2,1)}), bf16[2048,512]{0,1:T(8,128)(2,1)}) %all-gather.7.cloned.1.call-update) | async-done | bytes 2097168 | tf_op jit(solution)/shard_map/all_gather | solution.py:177
  84.5 31.3 %all-gather.9.cloned.1.call-done = bf16[2048,2,256]{0,2,1:T(8,128)(2,1)} async-done(((bf16[256,2,256]{0,2,1:T(8,128)(2,1)}), bf16[2048,2,256]{0,2,1:T(8,128)(2,1)}) %all-gather.9.cloned.1.call-update) | async-done | bytes 2097168 | tf_op jit(solution)/shard_map/all_gather | solution.py:178
  117.0 14.4 %while.24 = (s32[]{:T(128)}, f32[2,256,2]{1,2,0:T(2,128)S(1)}, f32[2,256,2]{1,2,0:T(2,128)S(1)}, f32[2,256,2,256]{3,1,0,2:T(8,128)S(1)}, f32[2,256,4]{1,2,0:T(4,...) while((s32[]{:T(128)}, f32[2,256,2]{1,2,0:T(2,128)S(1)}, ...), condition=%wide.region_7.8_spmd.clone, body=%wide.region_0.7_spmd.clone.sunk | while | flops 1640242432 | bytes 75457112 | solution.py:200
  117.0 14.4 %conditional.3 = ((f32[2,256,2]{1,2,0:T(2,128)S(1)}, f32[2,256,2]{1,2,0:T(2,128)S(1)}, f32[2,256,2,256]{3,1,0,2:T(8,128)S(1)}, f32[2,256,4]{1,2,0:T(4,128)S(1)},...) conditional(s32[]{:T(128)} %convert_element_type.151, (f32[2,256,2]{1,2,0:T(2,128)S(1)}, ...), branch_computations={%region_1.1_spmd, %region_2.6_spmd} | conditional | flops 1640242432 | bytes 75455728 | solution.py:197
  117.3 1.8 constant_dynamic-slice_fusion.1
  126.0 2.3 fusion.3
  128.4 2.0 fusion.21
  132.7 2.3 fusion.84
  136.4 1.6 copy.47
  140.8 1.7 fusion.34
  146.3 29.8 %reduce-scatter.3.cloned.1.call-done = bf16[128,2048]{1,0:T(8,128)(2,1)} async-done(((bf16[256,2048]{1,0:T(8,128)(2,1)}), bf16[128,2048]{1,0:T(8,128)(2,1)}) %reduce-scatter.3.cloned.1.call-update) | async-done | bytes 524304 | tf_op jit(solution)/shard_map/reduce_scatter | solution.py:203
  178.8 3.0 convolution_convert_fusion.1
  181.8 65.0 %all_to_all.10 = bf16[8,80,2048]{2,1,0:T(8,128)(2,1)} all-to-all(bf16[8,80,2048]{2,1,0:T(8,128)(2,1)} %bitcast.199), channel_id=1, replica_groups=mesh['grp'=2,'sp'=8,'tp'=2] {'sp'}, dimensions={0} | all-to-all | bytes 5242880 | tf_op jit(solution)/shard_map/all_to_all | solution.py:223
  246.9 66.6 %all-gather.11.cloned.1.call-done = bf16[1280,2048]{1,0:T(8,128)(2,1)} async-done(((bf16[640,2048]{1,0:T(8,128)(2,1)}), bf16[1280,2048]{1,0:T(8,128)(2,1)}) %all-gather.11.cloned.1.call-update) | async-done | bytes 5242896 | tf_op jit(solution)/shard_map/all_gather | solution.py:225
  313.5 10.2 %fusion.26 = f32[1280,1024]{1,0:T(8,128)} fusion(bf16[1280,2048]{1,0:T(8,128)(2,1)} %all-gather.11.cloned.1.call-done, bf16[1,2048,1024]{2,1,0:T(8,128)(2,1)} %param.41), kind=kOutput, calls=%fused_computation.34 | convolution fusion | flops 5368709120 | bytes 14680064 | tf_op jit(solution)/shard_map/dot_general | solution.py:226
  323.7 18.7 %convolution_convert_fusion = bf16[1280,2048]{1,0:T(8,128)(2,1)} fusion(bf16[1,1024,2048]{2,1,0:T(8,128)(2,1)} %param.43, f32[1280,1024]{1,0:T(8,128)} %fusion.26, bf16[1280,2048]{1,0:T(8,128)(2,1)} %all-gather.11.cloned.1.call-done, bf16[1,2048,1024]{2,1,0:T(8,128)(2,1)} %param.42), kind=kOutput, calls=%fused_computation.30 | convolution fusion | flops 10753146880 | bytes 24117248 | tf_op jit(solution)/shard_map/dot_general | solution.py:231
  342.4 65.9 %reduce-scatter.5.cloned.1.call-done = bf16[640,2048]{1,0:T(8,128)(2,1)} async-done(((bf16[1280,2048]{1,0:T(8,128)(2,1)}), bf16[640,2048]{1,0:T(8,128)(2,1)}) %reduce-scatter.5.cloned.1.call-update) | async-done | bytes 2621456 | tf_op jit(solution)/shard_map/reduce_scatter | solution.py:232
  408.3 4.8 all-to-all-start.1
  414.1 59.3 %all-to-all-done.1 = bf16[8,80,2048]{2,1,0:T(8,128)(2,1)} async-done(((bf16[8,80,2048]{2,1,0:T(8,128)(2,1)}), bf16[8,80,2048]{2,1,0:T(8,128)(2,1)}, u32[]{:S(2)}, u32[]{:S(2)}) %all-to-all-start.1) | async-done | bytes 2621472 | tf_op jit(solution)/shard_map/all_to_all | solution.py:234
  473.4 3.2 multiply_reduce_fusion
  (127 shorter events, 38.3 us)
Async XLA Ops:
  6.5 133.2 %copy-start = (bf16[512,2048]{1,0:T(8,128)(2,1)S(1)}, bf16[512,2048]{1,0:T(8,128)(2,1)}, u32[]{:S(2)}) copy-start(bf16[512,2048]{1,0:T(8,128)(2,1)} %param.33) | copy-start | bytes 6291460
  6.5 50.9 %all-gather.5.cloned.1.call-start = ((), (), s32[]{:S(2)}) async-start(), calls=%async_computation.4 | async-start | bytes 2359296 | tf_op jit(solution)/shard_map/all_gather | solution.py:176
  8.5 76.0 %all-gather.7.cloned.1.call-start = ((), (), s32[]{:S(2)}) async-start(), calls=%async_computation.5 | async-start | bytes 2359296 | tf_op jit(solution)/shard_map/all_gather | solution.py:177
  10.4 105.4 %all-gather.9.cloned.1.call-start = ((), (), s32[]{:S(2)}) async-start(), calls=%async_computation.6 | async-start | bytes 2359296 | tf_op jit(solution)/shard_map/all_gather | solution.py:178
  12.3 163.8 %reduce-scatter.3.cloned.1.call-start = ((), (), s32[]{:S(2)}) async-start(), calls=%async_computation.7 | async-start | bytes 1572864 | tf_op jit(solution)/shard_map/reduce_scatter | solution.py:203
  13.4 8.8 %collective-permute-start = (bf16[256,512]{0,1:T(8,128)(2,1)S(1)}, bf16[256,512]{0,1:T(8,128)(2,1)S(1)}, u32[]{:S(2)}, u32[]{:S(2)}) collective-permute-start(bf16[256,512]{0,1:T(8,128)(2,1)S(1)} %copy.41), channel_id=1, source_target_pairs={{0,2},{2,4},{4,6},{6,8},{8,10},{10,12},{12,14},{14,0},{1,3},{3,5},... | collective-permute-start | bytes 786440 | tf_op jit(solution)/shard_map/ppermute | solution.py:25
  14.0 14.9 %collective-permute-start.1 = (bf16[256,512]{0,1:T(8,128)(2,1)S(1)}, bf16[256,512]{0,1:T(8,128)(2,1)S(1)}, u32[]{:S(2)}, u32[]{:S(2)}) collective-permute-start(bf16[256,512]{0,1:T(8,128)(2,1)S(1)} %copy.41), channel_id=1, source_target_pairs={{0,14},{2,0},{4,2},{6,4},{8,6},{10,8},{12,10},{14,12},{1,15},{3,1}... | collective-permute-start | bytes 786440 | tf_op jit(solution)/shard_map/ppermute | solution.py:30
  22.3 16.4 %collective-permute-start.2 = (bf16[256,512]{0,1:T(8,128)(2,1)S(1)}, bf16[256,512]{0,1:T(8,128)(2,1)S(1)}, u32[]{:S(2)}, u32[]{:S(2)}) collective-permute-start(bf16[256,512]{0,1:T(8,128)(2,1)S(1)} %collective-permute-done), channel_id=1, source_target_pairs={{0,2},{2,4},{4,6},{6,8},{8,10},{10,12},{12,14},{14,0},{1,3},{3,5},... | collective-permute-start | bytes 786440 | tf_op jit(solution)/shard_map/ppermute | solution.py:25
  28.8 13.9 %collective-permute-start.3 = (bf16[256,512]{0,1:T(8,128)(2,1)S(1)}, bf16[256,512]{0,1:T(8,128)(2,1)S(1)}, u32[]{:S(2)}, u32[]{:S(2)}) collective-permute-start(bf16[256,512]{0,1:T(8,128)(2,1)S(1)} %collective-permute-done.1), channel_id=1, source_target_pairs={{0,14},{2,0},{4,2},{6,4},{8,6},{10,8},{12,10},{14,12},{1,15},{3,1}... | collective-permute-start | bytes 786440 | tf_op jit(solution)/shard_map/ppermute | solution.py:30
  38.7 8.9 %collective-permute-start.4 = (bf16[256,512]{0,1:T(8,128)(2,1)S(1)}, bf16[256,512]{0,1:T(8,128)(2,1)S(1)}, u32[]{:S(2)}, u32[]{:S(2)}) collective-permute-start(bf16[256,512]{0,1:T(8,128)(2,1)S(1)} %collective-permute-done.2), channel_id=1, source_target_pairs={{0,2},{2,4},{4,6},{6,8},{8,10},{10,12},{12,14},{14,0},{1,3},{3,5},... | collective-permute-start | bytes 786440 | tf_op jit(solution)/shard_map/ppermute | solution.py:25
  42.8 10.6 %collective-permute-start.5 = (bf16[256,512]{0,1:T(8,128)(2,1)S(1)}, bf16[256,512]{0,1:T(8,128)(2,1)S(1)}, u32[]{:S(2)}, u32[]{:S(2)}) collective-permute-start(bf16[256,512]{0,1:T(8,128)(2,1)S(1)} %collective-permute-done.3), channel_id=1, source_target_pairs={{0,14},{2,0},{4,2},{6,4},{8,6},{10,8},{12,10},{14,12},{1,15},{3,1}... | collective-permute-start | bytes 786440 | tf_op jit(solution)/shard_map/ppermute | solution.py:30
  47.5 9.1 %collective-permute-start.6 = (bf16[256,512]{0,1:T(8,128)(2,1)S(1)}, bf16[256,512]{0,1:T(8,128)(2,1)S(1)}, u32[]{:S(2)}, u32[]{:S(2)}) collective-permute-start(bf16[256,512]{0,1:T(8,128)(2,1)S(1)} %collective-permute-done.4), channel_id=1, source_target_pairs={{0,2},{2,4},{4,6},{6,8},{8,10},{10,12},{12,14},{14,0},{1,3},{3,5},... | collective-permute-start | bytes 786440 | tf_op jit(solution)/shard_map/ppermute | solution.py:25
  117.3 1.8 copy-start.2
  120.0 1.6 copy-start.1
  121.6 2.8 copy-start.3
  126.0 2.4 copy-start.4
  130.4 1.1 copy-start.5
  138.0 2.7 copy-start.6
  140.5 2.3 copy-start.11
  140.5 36.8 %copy-start.7 = (bf16[128,2048]{1,0:T(8,128)(2,1)S(1)}, bf16[128,2048]{1,0:T(8,128)(2,1)}, u32[]{:S(2)}) copy-start(bf16[128,2048]{1,0:T(8,128)(2,1)} %param.35) | copy-start | bytes 1572868
  140.5 36.8 %copy-start.8 = (f32[2048]{0:T(1024)S(1)}, f32[2048]{0:T(1024)}, u32[]{:S(2)}) copy-start(f32[2048]{0:T(1024)} %param.36) | copy-start | bytes 24580
  140.8 38.0 %copy-start.9 = (f32[2048]{0:T(1024)S(1)}, f32[2048]{0:T(1024)}, u32[]{:S(2)}) copy-start(f32[2048]{0:T(1024)} %param.37) | copy-start | bytes 24580
  142.5 171.0 %all-gather.11.cloned.1.call-start = ((), (), s32[]{:S(2)}) async-start(), calls=%async_computation.8 | async-start | bytes 7864320 | tf_op jit(solution)/shard_map/all_gather | solution.py:225
  246.8 161.5 %reduce-scatter.5.cloned.1.call-start = ((), (), s32[]{:S(2)}) async-start(), calls=%async_computation.9 | async-start | bytes 7864320 | tf_op jit(solution)/shard_map/reduce_scatter | solution.py:232
  342.4 70.7 %copy-start.12 = (f32[128,4]{0,1:T(4,128)S(1)}, f32[128,4]{0,1:T(4,128)}, u32[]{:S(2)}) copy-start(f32[128,4]{0,1:T(4,128)} %param.40) | copy-start | bytes 6148
  408.3 68.3 %copy-start.10 = (f32[2048]{0:T(1024)S(1)}, f32[2048]{0:T(1024)}, u32[]{:S(2)}) copy-start(f32[2048]{0:T(1024)} %param.38) | copy-start | bytes 24580
  408.3 65.1 %all-to-all-start.1 = ((bf16[8,80,2048]{2,1,0:T(8,128)(2,1)}), bf16[8,80,2048]{2,1,0:T(8,128)(2,1)}, u32[]{:S(2)}, u32[]{:S(2)}) async-start(bf16[8,80,2048]{2,1,0:T(8,128)(2,1)} %bitcast.202), calls=%async_computation.3 | async-start | bytes 5242880 | tf_op jit(solution)/shard_map/all_to_all | solution.py:234
Sparse Core Ops, SparseCore 0:
  8.9 44.2 all-gather.4
  54.8 29.6 all-gather.6
  86.1 29.6 all-gather.8
  142.6 33.3 reduce-scatter.2
  246.9 66.5 all-gather.10
  342.5 65.7 reduce-scatter.4
